TPU v7x, 32 devices: a whole 2x2x4 slice. The times are simulated.
32 devices in a mesh: grp: 2 (over y), sp: 4 (over z), tp: 4 (over x, core).
Axes of the slice: x: 2, y: 2, z: 4, core: 2. Of those that a mesh axis runs over, the one named last changes fastest.
Arguments:
- query_rows: bfloat16 [1024, 1024], P(('grp', 'sp'), 'tp'), parts along dimension 0, may hold values from -6 to 6
- key_rows: bfloat16 [1024, 1024], P(('grp', 'sp'), 'tp'), parts along dimension 0, may hold values from -6 to 6
- value_rows: bfloat16 [1024, 1024], P(('grp', 'sp'), 'tp'), parts along dimension 0, may hold values from -6 to 6
- gate_rows: bfloat16 [1024, 1024], P(('grp', 'sp'), 'tp'), parts along dimension 0, may hold values from -6 to 6
- log_decay: float32 [2, 8, 1024], P(None, 'tp', ('grp', 'sp')), parts along dimension 2, may hold values from -2 to 0, as said below
- head_gain: float32 [2, 1024], P(None, 'tp'), may hold values from 0.1 to 1.9
- out_weight: bfloat16 [1024, 2048], P('tp'), may hold values from -0.1875 to 0.1875
- residual: bfloat16 [1024, 2048], P(('grp', 'sp')), parts along dimension 0, may hold values from -6 to 6
- norm_gain: bfloat16 [2048], replicated, may hold values from 0.099609375 to 1.8984375
- gate_weight: bfloat16 [2048, 5632], P('sp', 'tp'), may hold values from -0.125 to 0.125
- up_weight: bfloat16 [2048, 5632], P('sp', 'tp'), may hold values from -0.125 to 0.125
- down_weight: bfloat16 [2048, 5632], P('sp', 'tp'), may hold values from -0.078125 to 0.078125
- gate_taps: bfloat16 [3, 5632], P(None, 'tp'), may hold values from -3.5 to 3.5
- up_taps: bfloat16 [3, 5632], P(None, 'tp'), may hold values from -3.5 to 3.5
Outputs:
- block_out: bfloat16 [1024, 2048], P(('grp', 'sp', 'tp')), parts along dimension 0
There are 2 independent parts, one for each index of `grp`. A program takes and returns all parts, laid end to end along the dimension named above; an argument that names none is the same for every part. Nothing has to cross between parts.
Inputs may be any that keep to these rules, and one draw needn't show every extreme that they name: `log_decay`: every entry is negative.
All inputs are finite; a program needn't handle non-finite values.
Results may differ from a plain program's by a relative error of at most 0.017.
Values may be sent and summed in bfloat16 or wider, within the bound.
A program may use at most 64 MiB of HBM per device.

v0:
```python
import math
import jax
import jax.numpy as jnp
from jax import lax
from jax.sharding import PartitionSpec as P

HEAD = 128
FULL_PRECISION = lax.Precision.HIGHEST
GROUP_EPS = 1e-05
NORM_EPS = 1e-06


def prefix(value, axis, join, neutral, backward):
    count, mine = (lax.axis_size(axis), lax.axis_index(axis))
    pieces = jax.tree.map(lambda part: lax.all_gather(part, axis), value)
    if backward:
        pieces = jax.tree.map(lambda part: part[::-1], pieces)
        mine = count - 1 - mine
    running = jax.tree.map(
        lambda part, zero: jnp.full_like(part, 0) + jnp.asarray(zero, part.dtype), value, neutral
    )

    def lap(position, running):
        longer = join(running, jax.tree.map(lambda part: part[position], pieces))
        return jax.tree.map(lambda new, old: jnp.where(position < mine, new, old), longer, running)

    return lax.fori_loop(0, count - 1, lap, running)


def padded_2(shard, sides, width):
    for axis, dim in sides:
        size, length = (lax.axis_size(axis), shard.shape[dim])
        up = [(i, (i + 1) % size) for i in range(size - 1)]
        down = [(j, i) for i, j in up]
        last = lax.slice_in_dim(shard, length - width, length, axis=dim)
        initial = lax.slice_in_dim(shard, 0, width, axis=dim)
        before = lax.ppermute(last, axis, up)
        after = lax.ppermute(initial, axis, down)
        shard = jnp.concatenate([before, shard, after], axis=dim)
    return shard


def state_combine(earlier, later):
    return (earlier[0] * later[0], earlier[1] * later[0][:, None, None] + later[1])


def group_norm(values):
    length, head_count, head_width = values.shape
    centre = values - jnp.mean(values, axis=2, keepdims=True)
    spread = jnp.mean(centre * centre, axis=2, keepdims=True)
    return (centre * lax.rsqrt(spread + GROUP_EPS)).reshape(length, head_count * head_width)


def rms_scale(middle, gain):
    values = middle.astype(jnp.float32)
    multiplier = lax.rsqrt(jnp.mean(values * values, axis=1, keepdims=True) + NORM_EPS)
    return (values * multiplier * gain.astype(jnp.float32)).astype(jnp.bfloat16)


def local_retention(query_all, key_all, value_all, log_rates):
    length, head_count, head_width = query_all.shape
    block_len = math.gcd(length, 512)
    block_count = length // block_len
    cumul = jnp.cumsum(log_rates, axis=1).T
    query_block = query_all.reshape(block_count, block_len, head_count, head_width)
    key_block = key_all.reshape(block_count, block_len, head_count, head_width)
    value_block = value_all.reshape(block_count, block_len, head_count, head_width)
    cumul_block = cumul.reshape(block_count, block_len, head_count)
    before = jnp.concatenate(
        [jnp.zeros((1, head_count), jnp.float32), cumul_block[:-1, -1]], axis=0
    )
    local_cumul = cumul_block - before[:, None, :]
    gap_logs = local_cumul[:, :, None, :] - local_cumul[:, None, :, :]
    lower_mask = (jnp.arange(block_len)[:, None] >= jnp.arange(block_len)[None, :])[
        None, :, :, None
    ]
    decay_mask = jnp.where(lower_mask, jnp.exp(jnp.minimum(gap_logs, 0.0)), 0.0)
    scores = (
        jnp.einsum("bthd,bshd->btsh", query_block, key_block, precision=FULL_PRECISION) * decay_mask
    )
    inner_part = jnp.einsum("btsh,bshe->bthe", scores, value_block, precision=FULL_PRECISION)
    to_end = jnp.exp(local_cumul[:, -1:, :] - local_cumul)
    block_states = jnp.einsum(
        "bshd,bshe->bhde", key_block * to_end[..., None], value_block, precision=FULL_PRECISION
    )
    block_decay = jnp.exp(local_cumul[:, -1, :])

    def carry_step(carry_state, inputs):
        return (carry_state * inputs[0][:, None, None] + inputs[1], carry_state)

    zero_state = jnp.zeros((head_count, head_width, head_width), jnp.float32)
    end_state, entering = lax.scan(carry_step, zero_state, (block_decay, block_states))
    carried = jnp.einsum(
        "bthd,bhde->bthe",
        query_block * jnp.exp(local_cumul)[..., None],
        entering,
        precision=FULL_PRECISION,
    )
    output = (inner_part + carried).reshape(length, head_count, head_width)
    return (output, end_state, cumul, jnp.exp(cumul[-1]))


def with_incoming(output, query_all, cumul, incoming):
    return output + jnp.einsum(
        "thd,hde->the", query_all * jnp.exp(cumul)[:, :, None], incoming, precision=FULL_PRECISION
    )


def shards(
    query_rows,
    key_rows,
    value_rows,
    gate_rows,
    log_decay,
    head_gain,
    out_weight,
    residual,
    norm_gain,
    gate_weight,
    up_weight,
    down_weight,
    gate_taps,
    up_taps,
):
    pair_local = jnp.concatenate([gate_weight, up_weight], axis=1)
    row_count = query_rows.shape[0]
    head_count = query_rows.shape[1] // HEAD
    key_scale = HEAD ** (-0.5)
    query_all = query_rows.astype(jnp.float32).reshape(row_count, head_count, HEAD)
    key_all = key_rows.astype(jnp.float32).reshape(row_count, head_count, HEAD) * key_scale
    value_all = value_rows.astype(jnp.float32).reshape(row_count, head_count, HEAD)
    identity = (
        jnp.ones((head_count,), jnp.float32),
        jnp.zeros((head_count, HEAD, HEAD), jnp.float32),
    )
    ahead_local, ahead_state, ahead_cumul, ahead_decay = local_retention(
        query_all, key_all, value_all, log_decay[0]
    )
    query_back = query_all[::-1]
    behind_local, behind_state, behind_cumul, behind_decay = local_retention(
        query_back, key_all[::-1], value_all[::-1], log_decay[1][:, ::-1]
    )
    ahead_in = prefix((ahead_decay, ahead_state), "sp", state_combine, identity, False)[1]
    behind_in = prefix((behind_decay, behind_state), "sp", state_combine, identity, True)[1]
    ahead_out = with_incoming(ahead_local, query_all, ahead_cumul, ahead_in)
    behind_out = with_incoming(behind_local, query_back, behind_cumul, behind_in)[::-1]
    combined = group_norm(ahead_out) * head_gain[0] + group_norm(behind_out) * head_gain[1]
    mixed_heads = (jax.nn.silu(gate_rows.astype(jnp.float32)) * combined).astype(jnp.bfloat16)
    gathered = (
        lax.all_gather(pair_local, "sp", axis=0, tiled=True),
        lax.all_gather(down_weight, "sp", axis=0, tiled=True),
    )
    pair_full, down_full = gathered
    share_rows = row_count // lax.axis_size("tp")
    own_start = lax.axis_index("tp") * share_rows
    picked = mixed_heads
    attended = lax.psum_scatter(
        jnp.dot(picked, out_weight, preferred_element_type=jnp.float32).astype(jnp.bfloat16),
        "tp",
        scatter_dimension=0,
        tiled=True,
    ).astype(jnp.float32)
    residual_own = lax.dynamic_slice_in_dim(residual, own_start, share_rows, 0)
    middle_own = lax.optimization_barrier(
        (residual_own.astype(jnp.float32) + attended).astype(jnp.bfloat16)
    )
    normed = rms_scale(middle_own, norm_gain)
    pre_both = jnp.dot(
        lax.all_gather(normed, "tp", axis=0, tiled=True),
        pair_full,
        preferred_element_type=jnp.float32,
    ).astype(jnp.bfloat16)
    padded = padded_2(pre_both, (("sp", 0),), 1)
    half_width = gate_taps.shape[1]
    tap_table = jnp.concatenate([gate_taps, up_taps], axis=1).astype(jnp.float32)
    conv_out = (
        tap_table[0] * padded[:-2].astype(jnp.float32)
        + tap_table[1] * padded[1:-1].astype(jnp.float32)
        + tap_table[2] * padded[2:].astype(jnp.float32)
    )
    hidden = (jax.nn.silu(conv_out[:, :half_width]) * conv_out[:, half_width:]).astype(jnp.bfloat16)
    picked = hidden
    ff_out = lax.psum_scatter(
        lax.dot_general(
            picked, down_full, (((1,), (1,)), ((), ())), preferred_element_type=jnp.float32
        ).astype(jnp.bfloat16),
        "tp",
        scatter_dimension=0,
        tiled=True,
    ).astype(jnp.float32)
    return (middle_own.astype(jnp.float32) + ff_out).astype(jnp.bfloat16)


def solution(mesh):
    in_specs = (
        P(("grp", "sp"), "tp"),
        P(("grp", "sp"), "tp"),
        P(("grp", "sp"), "tp"),
        P(("grp", "sp"), "tp"),
        P(None, "tp", ("grp", "sp")),
        P(None, "tp"),
        P("tp", None),
        P(("grp", "sp"), None),
        P(),
        P("sp", "tp"),
        P("sp", "tp"),
        P("sp", "tp"),
        P(None, "tp"),
        P(None, "tp"),
    )
    out_specs = P(("grp", "sp", "tp"), None)
    return jax.shard_map(shards, mesh=mesh, in_specs=in_specs, out_specs=out_specs, check_vma=False)
```

profile of v0, /device:TPU:0, one launch (start us, length us, event | category | flops | bytes accessed | tf_op | source)
XLA Modules:
  0.0 416.1 jit_solution(4977097718532471524)
XLA Ops:
  7.4 0.8 slice_bitcast_fusion.1
  8.2 0.3 reduce_window_sum.17
  8.5 0.2 slice_reduce_fusion.1
  8.9 0.3 reduce_window_sum.18
  9.2 0.2 slice_reduce_fusion
  9.4 1.0 copy.89
  10.4 0.2 reverse.3
  10.6 0.9 bitcast_convert_fusion
  11.5 1.0 convolution_add_fusion
  12.5 17.5 %all-gather = f32[8,128,128]{2,1,0:T(8,128)S(1)} all-gather(f32[2,128,128]{2,1,0:T(8,128)S(1)} %convolution_add_fusion), channel_id=2, replica_groups=mesh['grp'=2,'sp'=4,'tp'=4] {'sp'}, dimensions={0}, use_global_device_ids=true | all-gather | bytes 655360 | tf_op jit(solution)/shard_map/all_gather | solution.py:15
  30.0 0.2 exponential_reduce_fusion.1
  30.2 11.7 %all-gather.2 = f32[4,1,2]{2,1,0:T(1,128)S(1)} all-gather(f32[1,1,2]{2,1,0:T(1,128)S(1)} %bitcast.179), channel_id=1, replica_groups=mesh['grp'=2,'sp'=4,'tp'=4] {'sp'}, dimensions={0}, use_global_device_ids=true | all-gather | bytes 40 | tf_op jit(solution)/shard_map/all_gather | solution.py:15
  41.9 0.4 while.18
  42.3 0.5 fusion.33
  42.7 0.4 convolution_bitcast_fusion.3
  43.2 0.3 fusion.9
  43.5 0.3 fusion.62
  43.9 0.3 convolution_add_fusion.1
  44.2 15.1 %all-gather.1 = f32[8,128,128]{2,1,0:T(8,128)S(1)} all-gather(f32[2,128,128]{2,1,0:T(8,128)S(1)} %convolution_add_fusion.1), channel_id=3, replica_groups=mesh['grp'=2,'sp'=4,'tp'=4] {'sp'}, dimensions={0}, use_global_device_ids=true | all-gather | bytes 655360 | tf_op jit(solution)/shard_map/all_gather | solution.py:15
  59.4 0.2 exponential_reduce_fusion
  59.6 8.0 %all-gather.3 = f32[4,1,2]{2,1,0:T(1,128)S(1)} all-gather(f32[1,1,2]{2,1,0:T(1,128)S(1)} %bitcast.180), channel_id=1, replica_groups=mesh['grp'=2,'sp'=4,'tp'=4] {'sp'}, dimensions={0}, use_global_device_ids=true | all-gather | bytes 40 | tf_op jit(solution)/shard_map/all_gather | solution.py:15
  67.9 0.4 while.19
  68.3 0.4 fusion.11
  68.7 0.3 fusion.30
  69.0 0.3 convolution_bitcast_fusion
  69.4 0.4 fusion.7
  69.8 0.1 reduce_sum.47
  70.0 0.2 multiply_reduce_fusion
  70.2 0.1 subtract_multiply_fusion
  70.5 0.1 copy.58
  70.6 0.1 fusion.28
  70.7 1.1 convolution_convert_fusion.1
  72.0 3.1 pad_maximum_fusion
  75.2 0.5 all-gather.9.cloned.1.call-update
  75.8 17.1 %reduce-scatter.3.cloned.1.call-done = bf16[32,2048]{1,0:T(8,128)(2,1)} async-done(((bf16[128,2048]{1,0:T(8,128)(2,1)}), bf16[32,2048]{1,0:T(8,128)(2,1)}) %reduce-scatter.3.cloned.1.call-update) | async-done | bytes 131088 | tf_op jit(solution)/shard_map/reduce_scatter | solution.py:157
  92.9 1.0 add_convert_fusion
  93.9 0.1 fusion.15
  94.2 6.6 %all_gather.29 = bf16[128,2048]{1,0:T(8,128)(2,1)S(1)} all-gather(bf16[32,2048]{1,0:T(8,128)(2,1)S(1)} %fusion.17), channel_id=1, replica_groups=mesh['grp'=2,'sp'=4,'tp'=4] {'tp'}, dimensions={0}, use_global_device_ids=true | all-gather | bytes 655360 | tf_op jit(solution)/shard_map/all_gather | solution.py:169
  100.8 174.5 %all-gather.7.cloned.1.call-done = bf16[2048,2816]{1,0:T(8,128)(2,1)} async-done(((bf16[512,2816]{1,0:T(8,128)(2,1)}), bf16[2048,2816]{1,0:T(8,128)(2,1)}) %all-gather.7.cloned.1.call-update) | async-done | bytes 11534352 | tf_op jit(solution)/shard_map/all_gather | solution.py:150
  275.3 5.9 %convolution_convert_fusion = bf16[128,2816]{1,0:T(8,128)(2,1)S(1)} fusion(bf16[128,2048]{1,0:T(8,128)(2,1)S(1)} %all_gather.29, bf16[2048,2816]{1,0:T(8,128)(2,1)} %all-gather.7.cloned.1.call-done), kind=kOutput, calls=%fused_computation.6 | convolution fusion | flops 1476755456 | bytes 12779520 | tf_op jit(solution)/shard_map/dot_general | solution.py:168
  281.3 1.3 collective-permute-start
  282.6 1.3 collective-permute-start.1
  284.1 4.6 %collective-permute-done.1 = bf16[1,2816]{1,0:T(2,128)(2,1)S(1)} collective-permute-done((bf16[1,2816]{1,0:T(2,128)(2,1)S(1)}, bf16[1,2816]{1,0:T(2,128)(2,1)S(1)}, u32[]{:S(2)}, u32[]{:S(2)}) %collective-permute-start.1) | collective-permute-done | bytes 5664 | tf_op jit(solution)/shard_map/ppermute | solution.py:38
  288.7 0.5 multiply_add_fusion
  289.2 92.5 %all-gather.9.cloned.1.call-done = bf16[2048,1408]{1,0:T(8,128)(2,1)} async-done(((bf16[512,1408]{1,0:T(8,128)(2,1)}), bf16[2048,1408]{1,0:T(8,128)(2,1)}) %all-gather.9.cloned.1.call-update) | async-done | bytes 5767184 | tf_op jit(solution)/shard_map/all_gather | solution.py:151
  381.7 5.4 %convolution_convert_fusion.2 = bf16[128,2048]{1,0:T(8,128)(2,1)} fusion(bf16[2048,1408]{1,0:T(8,128)(2,1)} %all-gather.9.cloned.1.call-done, f32[128,2816]{1,0:T(8,128)S(1)} %multiply_add_fusion), kind=kOutput, calls=%fused_computation.9 | convolution fusion | flops 739540992 | bytes 7733248 | tf_op jit(solution)/shard_map/dot_general | solution.py:184
  387.1 20.0 %reduce-scatter.5.cloned.1.call-done = bf16[32,2048]{1,0:T(8,128)(2,1)} async-done(((bf16[128,2048]{1,0:T(8,128)(2,1)}), bf16[32,2048]{1,0:T(8,128)(2,1)}) %reduce-scatter.5.cloned.1.call-update) | async-done | bytes 131088 | tf_op jit(solution)/shard_map/reduce_scatter | solution.py:183
  407.1 1.6 fusion.18
  (67 shorter events, 2.1 us)
Async XLA Ops:
  7.4 63.4 %copy-start = (bf16[256,2048]{1,0:T(8,128)(2,1)S(1)}, bf16[256,2048]{1,0:T(8,128)(2,1)}, u32[]{:S(2)}) copy-start(bf16[256,2048]{1,0:T(8,128)(2,1)} %param.24) | copy-start | bytes 3145732
  7.4 85.6 %reduce-scatter.3.cloned.1.call-start = ((), (), s32[]{:S(2)}) async-start(), calls=%async_computation.2 | async-start | bytes 655360 | tf_op jit(solution)/shard_map/reduce_scatter | solution.py:157
  12.5 29.7 %copy-start.2 = (bf16[128,256]{1,0:T(8,128)(2,1)S(1)}, bf16[128,256]{1,0:T(8,128)(2,1)}, u32[]{:S(2)}) copy-start(bf16[128,256]{1,0:T(8,128)(2,1)} %param.18) | copy-start | bytes 196612
  41.9 1.6 copy-start.3
  68.3 2.1 copy-start.8
  68.3 2.1 copy-start.4
  70.3 1.6 copy-start.1
  71.9 203.4 %all-gather.7.cloned.1.call-start = ((), (), s32[]{:S(2)}) async-start(), calls=%async_computation.3 | async-start | bytes 14417920 | tf_op jit(solution)/shard_map/all_gather | solution.py:150
  75.1 0.7 copy-start.7
  75.1 306.6 %all-gather.9.cloned.1.call-start = ((), (), s32[]{:S(2)}) async-start(), calls=%async_computation.4 | async-start | bytes 7208960 | tf_op jit(solution)/shard_map/all_gather | solution.py:151
  75.7 331.4 %reduce-scatter.5.cloned.1.call-start = ((), (), s32[]{:S(2)}) async-start(), calls=%async_computation.5 | async-start | bytes 655360 | tf_op jit(solution)/shard_map/reduce_scatter | solution.py:183
  100.8 183.1 %copy-start.5 = (bf16[3,1408]{1,0:T(4,128)(2,1)S(1)}, bf16[3,1408]{1,0:T(4,128)(2,1)}, u32[]{:S(2)}) copy-start(bf16[3,1408]{1,0:T(4,128)(2,1)} %param.31) | copy-start | bytes 25348
  100.8 183.1 %copy-start.6 = (bf16[3,1408]{1,0:T(4,128)(2,1)S(1)}, bf16[3,1408]{1,0:T(4,128)(2,1)}, u32[]{:S(2)}) copy-start(bf16[3,1408]{1,0:T(4,128)(2,1)} %param.30) | copy-start | bytes 25348
  281.3 2.7 collective-permute-start
  282.6 6.0 %collective-permute-start.1 = (bf16[1,2816]{1,0:T(2,128)(2,1)S(1)}, bf16[1,2816]{1,0:T(2,128)(2,1)S(1)}, u32[]{:S(2)}, u32[]{:S(2)}) collective-permute-start(bf16[1,2816]{1,0:T(2,128)(2,1)S(1)} %get-tuple-element.315), channel_id=1, source_target_pairs={{4,0},{8,4},{12,8},{5,1},{9,5},{13,9},{6,2},{10,6},{14,10},{7,3},{... | collective-permute-start | bytes 16904 | tf_op jit(solution)/shard_map/ppermute | solution.py:38
Sparse Core Ops, SparseCore 0:
  72.0 20.8 reduce-scatter.2
  387.2 19.8 reduce-scatter.4
Sparse Core Ops, SparseCore 1:
  75.2 200.1 all-gather.6
  276.8 104.8 all-gather.8
where the time goes:
time: 417 us; the launch traced here: 416 us
  waiting for transfers between devices  309 us (74%)
  blocking collectives  58.9 us (14%)
  matrix products  16.7 us (4%)
  between operations  15.2 us (4%)
  other arithmetic  9.4 us (2%)
    all_gather x1, waiting for transfers between devices, shards(): lax.all_gather(pair_local, 'sp', axis=0, tiled=True)  175 us
    all_gather x1, waiting for transfers between devices, shards(): lax.all_gather(down_weight, 'sp', axis=0, tiled=True)  92.5 us
    all_gather x4, blocking collectives, prefix(): pieces = jax.tree.map(lambda part: lax.all_gather(part, axis), value)  52.3 us
    reduce_scatter x1, waiting for transfers between devices, shards(): lax.psum_scatter(lax.dot_general(picked, down_full, (((1,), (1,)), ((), (...  20 us
    reduce_scatter x1, waiting for transfers between devices, shards(): lax.psum_scatter(jnp.dot(picked, out_weight, preferred_element_type=jnp.f...  17.1 us
  transfers between devices with their start and end apart: 6, of which 5 were waited for; matrix products, arithmetic and copies ran while one was open for 3% of the time, Pallas kernels for 0%

commit v1 on v0

--- a/solution.py
+++ b/solution.py
@@ -8,6 +8,11 @@
 FULL_PRECISION = lax.Precision.HIGHEST
 GROUP_EPS = 1e-05
 NORM_EPS = 1e-06
+
+
+def exchange_gather(shard, axis, dim):
+    stack = jnp.stack([shard] * lax.axis_size(axis))
+    return jnp.concatenate(lax.all_to_all(stack, axis, 0, 0), axis=dim)
 
 
 def prefix(value, axis, join, neutral, backward):
@@ -147,7 +152,7 @@
     combined = group_norm(ahead_out) * head_gain[0] + group_norm(behind_out) * head_gain[1]
     mixed_heads = (jax.nn.silu(gate_rows.astype(jnp.float32)) * combined).astype(jnp.bfloat16)
     gathered = (
-        lax.all_gather(pair_local, "sp", axis=0, tiled=True),
+        exchange_gather(pair_local, "sp", 0),
         lax.all_gather(down_weight, "sp", axis=0, tiled=True),
     )
     pair_full, down_full = gathered

time: 417 us -> 469 us (1.12)
  blocking collectives: 58.9 us -> 299 us
  waiting for transfers between devices: 309 us -> 108 us
  starting transfers between devices: 2.71 us -> 11.2 us
  local copies, waits for them, and re-layouts: 3.67 us -> 8.91 us
    all_gather x4, blocking collectives: 52.3 us -> 293 us  [prefix(): pieces = jax.tree.map(lambda part: lax.all_gather(part, axis), value)]
    all_gather x1 -> x0, waiting for transfers between devices: 175 us -> none  [shards(): lax.all_gather(pair_local, 'sp', axis=0, tiled=True)]
    all_gather x1, waiting for transfers between devices: 92.5 us -> 61.3 us  [shards(): lax.all_gather(down_weight, 'sp', axis=0, tiled=True)]
    another operation x1 -> x2, local copies, waits for them, and re-layouts: 0.18 us -> 7.09 us  [the longest x1 6.91 us: exchange_gather(): stack = jnp.stack([shard] * lax.axis_size(axis))]
    all_to_all x0 -> x1, starting transfers between devices: none -> 6.48 us  [exchange_gather(): return jnp.concatenate(lax.all_to_all(stack, axis, 0, 0), axis=dim)]
where the time goes in v1:
time: 469 us; the launch traced here: 468 us
  blocking collectives  299 us (64%)
  waiting for transfers between devices  108 us (23%)
  matrix products  15.9 us (3%)
  between operations  15.2 us (3%)
  starting transfers between devices  11.2 us (2%)
  other arithmetic  9.15 us (2%)
  local copies, waits for them, and re-layouts  8.91 us (2%)
    all_gather x4, blocking collectives, prefix(): pieces = jax.tree.map(lambda part: lax.all_gather(part, axis), value)  293 us
    all_gather x1, waiting for transfers between devices, shards(): lax.all_gather(down_weight, 'sp', axis=0, tiled=True)  61.3 us
    reduce_scatter x1, waiting for transfers between devices, shards(): lax.psum_scatter(lax.dot_general(picked, down_full, (((1,), (1,)), ((), (...  20.1 us
    reduce_scatter x1, waiting for transfers between devices, shards(): lax.psum_scatter(jnp.dot(picked, out_weight, preferred_element_type=jnp.f...  19.8 us
  transfers between devices with their start and end apart: 6, of which 5 were waited for; matrix products, arithmetic and copies ran while one was open for 3% of the time, Pallas kernels for 0%

profile of v1, /device:TPU:0, one launch (start us, length us, event | category | flops | bytes accessed | tf_op | source)
XLA Modules:
  0.0 468.4 jit_solution(864635782819887003)
XLA Ops:
  7.4 3.7 pad_maximum_fusion
  11.1 6.9 %stack.2 = bf16[4,512,2816]{2,1,0:T(8,128)(2,1)} broadcast(bf16[512,2816]{1,0:T(8,128)(2,1)} %pad_maximum_fusion), dimensions={1,2} | broadcast | bytes 14417920 | tf_op jit(solution)/shard_map/stack | solution.py:14
  18.0 6.5 %all-to-all-start = ((bf16[4,512,2816]{2,1,0:T(8,128)(2,1)}), bf16[4,512,2816]{2,1,0:T(8,128)(2,1)}, u32[]{:S(2)}, u32[]{:S(2)}) async-start(bf16[4,512,2816]{2,1,0:T(8,128)(2,1)} %stack.2), calls=%async_computation.1 | async-start | bytes 23068672 | tf_op jit(solution)/shard_map/all_to_all | solution.py:15
  24.5 0.3 reduce_window_sum.17
  24.8 0.2 exponential_reduce_fusion.1
  25.0 192.1 %all-gather.2 = f32[4,1,2]{2,1,0:T(1,128)S(1)} all-gather(f32[1,1,2]{2,1,0:T(1,128)S(1)} %bitcast.180), channel_id=1, replica_groups=mesh['grp'=2,'sp'=4,'tp'=4] {'sp'}, dimensions={0}, use_global_device_ids=true | all-gather | bytes 40 | tf_op jit(solution)/shard_map/all_gather | solution.py:20
  217.2 0.3 reduce_window_sum.18
  217.5 0.2 exponential_reduce_fusion
  217.7 70.3 %all-gather.3 = f32[4,1,2]{2,1,0:T(1,128)S(1)} all-gather(f32[1,1,2]{2,1,0:T(1,128)S(1)} %bitcast.181), channel_id=1, replica_groups=mesh['grp'=2,'sp'=4,'tp'=4] {'sp'}, dimensions={0}, use_global_device_ids=true | all-gather | bytes 40 | tf_op jit(solution)/shard_map/all_gather | solution.py:20
  288.1 0.2 reverse.3
  288.5 0.2 slice_reduce_fusion
  288.7 0.3 convolution_add_fusion.1
  289.0 14.9 %all-gather.1 = f32[8,128,128]{2,1,0:T(8,128)S(1)} all-gather(f32[2,128,128]{2,1,0:T(8,128)S(1)} %convolution_add_fusion.1), channel_id=3, replica_groups=mesh['grp'=2,'sp'=4,'tp'=4] {'sp'}, dimensions={0}, use_global_device_ids=true | all-gather | bytes 655360 | tf_op jit(solution)/shard_map/all_gather | solution.py:20
  304.4 0.4 fusion.11
  304.8 0.3 fusion.30
  305.1 0.4 while.19
  305.5 0.3 convolution_bitcast_fusion
  305.8 0.4 fusion.7
  306.3 0.1 reduce_sum.47
  306.4 0.2 multiply_reduce_fusion
  306.6 0.1 subtract_multiply_fusion
  306.9 0.1 copy.58
  307.0 0.2 slice_reduce_fusion.1
  307.2 0.3 fusion.9
  307.6 0.2 convolution_add_fusion
  307.8 15.5 %all-gather = f32[8,128,128]{2,1,0:T(8,128)S(1)} all-gather(f32[2,128,128]{2,1,0:T(8,128)S(1)} %convolution_add_fusion), channel_id=2, replica_groups=mesh['grp'=2,'sp'=4,'tp'=4] {'sp'}, dimensions={0}, use_global_device_ids=true | all-gather | bytes 655360 | tf_op jit(solution)/shard_map/all_gather | solution.py:20
  323.3 0.5 fusion.33
  323.8 0.4 while.18
  324.2 0.4 convolution_bitcast_fusion.3
  324.6 0.3 fusion.62
  325.0 0.1 fusion.28
  325.2 1.1 convolution_convert_fusion.1
  326.4 0.5 all-gather.6.cloned.1.call-update
  327.0 19.8 %reduce-scatter.3.cloned.1.call-done = bf16[32,2048]{1,0:T(8,128)(2,1)} async-done(((bf16[128,2048]{1,0:T(8,128)(2,1)}), bf16[32,2048]{1,0:T(8,128)(2,1)}) %reduce-scatter.3.cloned.1.call-update) | async-done | bytes 131088 | tf_op jit(solution)/shard_map/reduce_scatter | solution.py:162
  346.8 1.0 add_convert_fusion
  347.8 0.1 fusion.15
  348.0 0.1 fusion.17
  348.1 6.6 %all_gather.26 = bf16[128,2048]{1,0:T(8,128)(2,1)S(1)} all-gather(bf16[32,2048]{1,0:T(8,128)(2,1)S(1)} %fusion.17), channel_id=1, replica_groups=mesh['grp'=2,'sp'=4,'tp'=4] {'tp'}, dimensions={0}, use_global_device_ids=true | all-gather | bytes 655360 | tf_op jit(solution)/shard_map/all_gather | solution.py:174
  354.7 6.0 %convolution_convert_fusion = bf16[128,2816]{1,0:T(8,128)(2,1)S(1)} fusion(bf16[128,2048]{1,0:T(8,128)(2,1)S(1)} %all_gather.26, bf16[2048,2816]{1,0:T(8,128)(2,1)} %bitcast.30), kind=kOutput, calls=%fused_computation.6 | convolution fusion | flops 1476755456 | bytes 12779520 | tf_op jit(solution)/shard_map/dot_general | solution.py:173
  360.7 3.4 collective-permute-start
  364.1 1.3 collective-permute-start.1
  365.5 0.1 collective-permute-done
  365.7 6.4 %collective-permute-done.1 = bf16[1,2816]{1,0:T(2,128)(2,1)S(1)} collective-permute-done((bf16[1,2816]{1,0:T(2,128)(2,1)S(1)}, bf16[1,2816]{1,0:T(2,128)(2,1)S(1)}, u32[]{:S(2)}, u32[]{:S(2)}) %collective-permute-start.1) | collective-permute-done | bytes 5664 | tf_op jit(solution)/shard_map/ppermute | solution.py:43
  372.0 0.5 multiply_add_fusion
  372.5 61.3 %all-gather.6.cloned.1.call-done = bf16[2048,1408]{1,0:T(8,128)(2,1)} async-done(((bf16[512,1408]{1,0:T(8,128)(2,1)}), bf16[2048,1408]{1,0:T(8,128)(2,1)}) %all-gather.6.cloned.1.call-update) | async-done | bytes 5767184 | tf_op jit(solution)/shard_map/all_gather | solution.py:156
  433.9 5.4 %convolution_convert_fusion.2 = bf16[128,2048]{1,0:T(8,128)(2,1)} fusion(bf16[2048,1408]{1,0:T(8,128)(2,1)} %all-gather.6.cloned.1.call-done, f32[128,2816]{1,0:T(8,128)S(1)} %multiply_add_fusion), kind=kOutput, calls=%fused_computation.9 | convolution fusion | flops 739540992 | bytes 7733248 | tf_op jit(solution)/shard_map/dot_general | solution.py:189
  439.3 20.1 %reduce-scatter.5.cloned.1.call-done = bf16[32,2048]{1,0:T(8,128)(2,1)} async-done(((bf16[128,2048]{1,0:T(8,128)(2,1)}), bf16[32,2048]{1,0:T(8,128)(2,1)}) %reduce-scatter.5.cloned.1.call-update) | async-done | bytes 131088 | tf_op jit(solution)/shard_map/reduce_scatter | solution.py:188
  459.4 1.6 fusion.18
  (69 shorter events, 2.0 us)
Async XLA Ops:
  7.4 317.8 %copy-start = (bf16[256,2048]{1,0:T(8,128)(2,1)S(1)}, bf16[256,2048]{1,0:T(8,128)(2,1)}, u32[]{:S(2)}) copy-start(bf16[256,2048]{1,0:T(8,128)(2,1)} %param.24) | copy-start | bytes 3145732
  18.0 6.5 %copy-start.8 = (f32[2,2,128]{2,1,0:T(2,128)S(1)}, f32[2,2,128]{2,1,0:T(2,128)}, u32[]{:S(2)}) copy-start(f32[2,2,128]{2,1,0:T(2,128)} %param.22) | copy-start | bytes 6148
  18.0 270.0 %copy-start.3 = (bf16[128,256]{1,0:T(8,128)(2,1)S(1)}, bf16[128,256]{1,0:T(8,128)(2,1)}, u32[]{:S(2)}) copy-start(bf16[128,256]{1,0:T(8,128)(2,1)} %param.19) | copy-start | bytes 196612
  18.0 270.3 %copy-start.2 = (bf16[128,256]{1,0:T(8,128)(2,1)S(1)}, bf16[128,256]{1,0:T(8,128)(2,1)}, u32[]{:S(2)}) copy-start(bf16[128,256]{1,0:T(8,128)(2,1)} %param.20) | copy-start | bytes 196612
  18.0 336.6 %all-to-all-start = ((bf16[4,512,2816]{2,1,0:T(8,128)(2,1)}), bf16[4,512,2816]{2,1,0:T(8,128)(2,1)}, u32[]{:S(2)}, u32[]{:S(2)}) async-start(bf16[4,512,2816]{2,1,0:T(8,128)(2,1)} %stack.2), calls=%async_computation.1 | async-start | bytes 23068672 | tf_op jit(solution)/shard_map/all_to_all | solution.py:15
  24.5 322.3 %reduce-scatter.3.cloned.1.call-start = ((), (), s32[]{:S(2)}) async-start(), calls=%async_computation.3 | async-start | bytes 655360 | tf_op jit(solution)/shard_map/reduce_scatter | solution.py:162
  288.1 16.2 %copy-start.1 = (bf16[128,256]{1,0:T(8,128)(2,1)S(1)}, bf16[128,256]{1,0:T(8,128)(2,1)}, u32[]{:S(2)}) copy-start(bf16[128,256]{1,0:T(8,128)(2,1)} %param.18) | copy-start | bytes 196612
  305.5 1.4 copy-start.4
  323.8 1.2 copy-start.9
  325.2 1.8 copy-start.7
  326.3 107.5 %all-gather.6.cloned.1.call-start = ((), (), s32[]{:S(2)}) async-start(), calls=%async_computation.4 | async-start | bytes 7208960 | tf_op jit(solution)/shard_map/all_gather | solution.py:156
  326.9 132.4 %reduce-scatter.5.cloned.1.call-start = ((), (), s32[]{:S(2)}) async-start(), calls=%async_computation.5 | async-start | bytes 655360 | tf_op jit(solution)/shard_map/reduce_scatter | solution.py:188
  354.7 10.8 %copy-start.5 = (bf16[3,1408]{1,0:T(4,128)(2,1)S(1)}, bf16[3,1408]{1,0:T(4,128)(2,1)}, u32[]{:S(2)}) copy-start(bf16[3,1408]{1,0:T(4,128)(2,1)} %param.31) | copy-start | bytes 25348
  354.7 10.8 %copy-start.6 = (bf16[3,1408]{1,0:T(4,128)(2,1)S(1)}, bf16[3,1408]{1,0:T(4,128)(2,1)}, u32[]{:S(2)}) copy-start(bf16[3,1408]{1,0:T(4,128)(2,1)} %param.30) | copy-start | bytes 25348
  360.7 4.9 %collective-permute-start = (bf16[1,2816]{1,0:T(2,128)(2,1)S(1)}, bf16[1,2816]{1,0:T(2,128)(2,1)S(1)}, u32[]{:S(2)}, u32[]{:S(2)}) collective-permute-start(bf16[1,2816]{1,0:T(2,128)(2,1)S(1)} %get-tuple-element.314), channel_id=1, source_target_pairs={{0,4},{4,8},{8,12},{1,5},{5,9},{9,13},{2,6},{6,10},{10,14},{3,7},{... | collective-permute-start | bytes 16904 | tf_op jit(solution)/shard_map/ppermute | solution.py:42
  364.1 7.9 %collective-permute-start.1 = (bf16[1,2816]{1,0:T(2,128)(2,1)S(1)}, bf16[1,2816]{1,0:T(2,128)(2,1)S(1)}, u32[]{:S(2)}, u32[]{:S(2)}) collective-permute-start(bf16[1,2816]{1,0:T(2,128)(2,1)S(1)} %get-tuple-element.315), channel_id=1, source_target_pairs={{4,0},{8,4},{12,8},{5,1},{9,5},{13,9},{6,2},{10,6},{14,10},{7,3},{... | collective-permute-start | bytes 16904 | tf_op jit(solution)/shard_map/ppermute | solution.py:43
Sparse Core Ops, SparseCore 0:
  326.5 20.2 reduce-scatter.2
  439.4 19.9 reduce-scatter.4
Sparse Core Ops, SparseCore 1:
  328.4 105.4 all-gather.5
